TPU v7x, 32 devices: a whole 2x2x4 slice. The times are simulated.
32 devices in a mesh: sp: 16 (over z, y, core), tp: 2 (over x).
Axes of the slice: x: 2, y: 2, z: 4, core: 2. Of those that a mesh axis runs over, the one named last changes fastest.
Arguments:
- queries: bfloat16 [4096, 512], P('sp', 'tp'), may hold values from -8 to 8
- keys: bfloat16 [4096, 512], P('sp', 'tp'), may hold values from -8 to 8
- values: bfloat16 [4096, 512], P('sp', 'tp'), may hold values from -6 to 6
- score_shift: float32 [8], P('tp'), may hold values from 3 to 20
- resid: bfloat16 [4096, 2048], P(('sp', 'tp')), may hold values from -6 to 6
- w_out: bfloat16 [512, 2048], replicated, may hold values from -0.25 to 0.25
- gain_mix: float32 [2048], replicated, may hold values from 0.1 to 1.9
- gain_pre: float32 [2048], replicated, may hold values from 0.1 to 1.9
- w_gate: bfloat16 [2048, 5632], P('sp', 'tp'), may hold values from -0.125 to 0.125
- w_up: bfloat16 [2048, 5632], P('sp', 'tp'), may hold values from -0.125 to 0.125
- conv_gate: float32 [3, 5632], P(None, 'tp'), may hold values from -3 to 3
- conv_up: float32 [3, 5632], P(None, 'tp'), may hold values from -3 to 3
- w_down: bfloat16 [5632, 2048], P('tp', 'sp'), may hold values from -0.078125 to 0.078125
- gain_post: float32 [2048], replicated, may hold values from 0.1 to 1.9
Outputs:
- result: bfloat16 [4096, 2048], P(('sp', 'tp'))
All inputs are finite; a program needn't handle non-finite values.
Results may differ from a plain program's by a relative error of at most 0.017.
Values may be sent and summed in bfloat16 or wider, within the bound.
A program may use at most 128 MiB of HBM per device.

v0:
```python
import jax
import jax.numpy as jnp
from jax import lax
from jax.sharding import PartitionSpec as P

HEAD_DIM = 64
KERNEL = 3


def from_behind(x, axis, by):
    length = lax.axis_size(axis)
    pairs = [(i, i + by) for i in range(length) if 0 <= i + by < length]
    return lax.ppermute(x, axis, pairs)


def rms_scale(values_in):
    return values_in * lax.rsqrt(jnp.mean(values_in * values_in, axis=-1, keepdims=True) + 1e-06)


def collect_weights(w_gate, w_up, w_down):
    gate_whole, up_whole = (
        lax.all_gather(w_gate, "sp", axis=0, tiled=True),
        lax.all_gather(w_up, "sp", axis=0, tiled=True),
    )
    down_whole = lax.all_gather(w_down, "sp", axis=1, tiled=True)
    return (gate_whole, up_whole, down_whole)


def stick_attention(queries, key_whole, value_whole, score_shift):
    tok_rows = queries.shape[0]
    local_heads = queries.shape[1] // HEAD_DIM
    total = key_whole.shape[0]
    shards = total // tok_rows
    group = max(
        (
            factor
            for factor in range(1, shards + 1)
            if shards % factor == 0 and factor * tok_rows <= max(2048, tok_rows)
        )
    )
    span = group * tok_rows
    offset = lax.axis_index("sp") * tok_rows
    query_heads = queries.reshape(tok_rows, local_heads, HEAD_DIM)
    key_heads = key_whole.reshape(total, local_heads, HEAD_DIM)
    value_heads = value_whole.reshape(total, local_heads, HEAD_DIM)
    query_pos = offset + jnp.arange(tok_rows, dtype=jnp.int32)
    last_block = (offset + tok_rows - 1) // span

    def visit(turn, carry):
        accum, tail = carry
        block_start = (last_block - turn) * span
        key_block = lax.dynamic_slice_in_dim(key_heads, block_start, span, 0)
        value_block = lax.dynamic_slice_in_dim(value_heads, block_start, span, 0)
        scores = jnp.einsum(
            "qhd,khd->hqk", query_heads, key_block, preferred_element_type=jnp.float32
        )
        scores = scores * HEAD_DIM ** (-0.5) - score_shift[:, None, None]
        key_pos = block_start + jnp.arange(span, dtype=jnp.int32)
        causal = (key_pos[None, :] < query_pos[:, None])[None, :, :]
        log_keep = jnp.where(causal, -jax.nn.softplus(scores), 0.0)
        later = lax.cumsum(log_keep, axis=2, reverse=True) - log_keep
        weights = jnp.where(
            causal, jnp.exp(jax.nn.log_sigmoid(scores) + later + tail[:, :, None]), 0.0
        ).astype(jnp.bfloat16)
        accum = accum + jnp.einsum(
            "hqk,khd->hqd", weights, value_block, preferred_element_type=jnp.float32
        )
        return (accum, tail + jnp.sum(log_keep, axis=2))

    start_carry = (
        jnp.zeros((local_heads, tok_rows, HEAD_DIM), jnp.float32),
        jnp.zeros((local_heads, tok_rows), jnp.float32),
    )
    accum, _ = lax.fori_loop(0, last_block + 1, visit, start_carry)
    return accum.transpose(1, 0, 2).reshape(tok_rows, local_heads * HEAD_DIM).astype(jnp.bfloat16)


def local(
    queries,
    keys,
    values,
    score_shift,
    resid,
    w_out,
    gain_mix,
    gain_pre,
    w_gate,
    w_up,
    conv_gate,
    conv_up,
    w_down,
    gain_post,
):
    gate_whole, up_whole, down_whole = collect_weights(w_gate, w_up, w_down)
    key_whole, value_whole = (
        lax.all_gather(keys, "sp", axis=0, tiled=True),
        lax.all_gather(values, "sp", axis=0, tiled=True),
    )
    attended = stick_attention(queries, key_whole, value_whole, score_shift)
    head_rows = lax.all_to_all(attended, "tp", split_axis=0, concat_axis=1, tiled=True)
    mixed = jnp.dot(head_rows, w_out, preferred_element_type=jnp.float32).astype(jnp.bfloat16)
    middle = (resid.astype(jnp.float32) + gain_mix * rms_scale(mixed.astype(jnp.float32))).astype(
        jnp.bfloat16
    )
    normed = (gain_pre * rms_scale(middle.astype(jnp.float32))).astype(jnp.bfloat16)
    piece = lax.all_gather(normed, "tp", axis=0, tiled=True)
    gate_part = jnp.dot(piece, gate_whole, preferred_element_type=jnp.float32).astype(jnp.bfloat16)
    up_part = jnp.dot(piece, up_whole, preferred_element_type=jnp.float32).astype(jnp.bfloat16)
    projected = jnp.concatenate([gate_part, up_part], axis=1)
    tok_rows = projected.shape[0]
    local_units = projected.shape[1] // 2
    edge = from_behind(projected[tok_rows - (KERNEL - 1) :], "sp", 1)
    extended = jnp.concatenate([edge, projected], axis=0).astype(jnp.float32)
    taps = jnp.concatenate([conv_gate, conv_up], axis=1)
    convolved = taps[0] * extended[0:tok_rows]
    for tap in range(1, KERNEL):
        convolved = convolved + taps[tap] * extended[tap : tap + tok_rows]
    hidden = (jax.nn.silu(convolved[:, :local_units]) * convolved[:, local_units:]).astype(
        jnp.bfloat16
    )
    summed = lax.psum_scatter(
        jnp.dot(hidden, down_whole, preferred_element_type=jnp.float32).astype(jnp.bfloat16),
        "tp",
        scatter_dimension=0,
        tiled=True,
    )
    return (middle.astype(jnp.float32) + gain_post * rms_scale(summed.astype(jnp.float32))).astype(
        jnp.bfloat16
    )


def solution(mesh):
    in_specs = (
        P("sp", "tp"),
        P("sp", "tp"),
        P("sp", "tp"),
        P("tp"),
        P(("sp", "tp"), None),
        P(),
        P(),
        P(),
        P("sp", "tp"),
        P("sp", "tp"),
        P(None, "tp"),
        P(None, "tp"),
        P("tp", "sp"),
        P(),
    )
    out_specs = P(("sp", "tp"), None)
    return jax.shard_map(local, mesh=mesh, in_specs=in_specs, out_specs=out_specs, check_vma=False)
```

profile of v0, /device:TPU:0, one launch (start us, length us, event | category | flops | bytes accessed | tf_op | source)
XLA Modules:
  0.0 598.9 jit_solution(18021762310633869945)
XLA Ops:
  6.5 0.7 all-gather.7.cloned.1.call-update
  8.1 1.0 copy.38
  9.1 44.6 %all-gather.7.cloned.1.call-done = bf16[4096,256]{1,0:T(8,128)(2,1)} async-done(((bf16[256,256]{1,0:T(8,128)(2,1)}), bf16[4096,256]{1,0:T(8,128)(2,1)}) %all-gather.7.cloned.1.call-update) | async-done | bytes 2097168 | tf_op jit(solution)/shard_map/all_gather | solution.py:96
  53.7 4.1 copy.37
  57.8 38.3 %all-gather.9.cloned.1.call-done = bf16[4096,256]{1,0:T(8,128)(2,1)} async-done(((bf16[256,256]{1,0:T(8,128)(2,1)}), bf16[4096,256]{1,0:T(8,128)(2,1)}) %all-gather.9.cloned.1.call-update) | async-done | bytes 2097168 | tf_op jit(solution)/shard_map/all_gather | solution.py:97
  96.1 4.1 copy.39
  100.3 75.2 %while.13 = (s32[]{:T(128)}, f32[4,256,64]{1,2,0:T(8,128)S(1)}, f32[4,256]{1,0:T(4,128)S(1)}, s32[]{:T(128)}, s32[]{:T(128)}, /*index=5*/bf16[4096,4,64]{0,2,1:T...) while((s32[]{:T(128)}, f32[4,256,64]{1,2,0:T(8,128)S(1)}, ...), condition=%wide.region_4.5_spmd.clone, body=%wide.region_0.4_spmd.clone.sunk | while | flops 877462784 | bytes 139045168 | solution.py:74
  101.1 12.3 %fusion.55 = (f32[4,256]{1,0:T(4,128)S(1)}, f32[4,256,2048]{1,2,0:T(8,128)}, f32[4,2048,256]{2,1,0:T(8,128)}) fusion(f32[4]{0:T(128)S(1)} %get-tuple-element.218, pred[256,2048]{0,1:T(8,128)(4,1)S(1)} %broadcast_compare_fusion.2, bf16[256,4,64]{0,2,1:T(8,128)(2,1)S(1)} %get-tuple-element.217, bf16[4096,4,64]{0,2,1:T(8,128)(2,1)} %get-tuple-element.216, ...), kind=kOutput, calls=%fused_computation.33.clone.1 | convolution fusion | flops 291503104 | bytes 18485268 | tf_op jit(solution)/shard_map/while/body/qhd,khd->hqk/dot_general | solution.py:54
  113.3 24.0 %fusion.56 = f32[4,256,16,128]{1,2,3,0:T(8,128)S(1)} fusion(f32[4,256,16,128]{1,3,2,0:T(8,128)} %bitcast.63), kind=kOutput, calls=%fused_computation.19.clone.1 | output fusion | flops 266338304 | bytes 16777216 | tf_op jit(solution)/shard_map/reduce-window
  137.4 3.2 copy-done.1
  140.8 4.4 broadcast_add_fusion.2
  145.3 5.1 copy.47
  150.4 15.1 %fusion.57 = bf16[4,256,2048]{1,2,0:T(8,128)(2,1)S(1)} fusion(f32[4,256,16,128]{1,3,2,0:T(8,128)S(1)} %copy.47, f32[4,2048,256]{2,1,0:T(8,128)} %get-tuple-element.179, f32[4,256]{1,0:T(4,128)S(1)} %get-tuple-element.198, f32[4]{0:T(128)S(1)} %get-tuple-element.218, pred[256,2048]{0,1:T(8,128)(4,1)S(1)} %broadcast_compare_fusion.2), kind=kLoop, calls=%fused_computation.8.clone.1 | loop fusion | flops 48234496 | bytes 21499920 | tf_op jit(solution)/shard_map/while/body/convert_element_type | solution.py:64
  165.4 0.8 convolution_add_fusion.2
  175.6 7.0 %all_to_all.16 = bf16[2,128,256]{1,2,0:T(8,128)(2,1)S(1)} all-to-all(bf16[2,128,256]{1,2,0:T(8,128)(2,1)S(1)} %copy.40), channel_id=1, replica_groups=mesh['sp'=16,'tp'=2] {'tp'}, dimensions={0} | all-to-all | bytes 262144 | tf_op jit(solution)/shard_map/all_to_all | solution.py:100
  183.2 1.4 fusion.30
  184.6 0.8 copy-done.3
  185.4 1.0 fusion.32
  189.5 82.0 %all-gather.11.cloned.1.call-done = bf16[256,2048]{1,0:T(8,128)(2,1)} async-done(((bf16[128,2048]{1,0:T(8,128)(2,1)}), bf16[256,2048]{1,0:T(8,128)(2,1)}) %all-gather.11.cloned.1.call-update) | async-done | bytes 1048592 | tf_op jit(solution)/shard_map/all_gather | solution.py:106
  271.5 96.2 %all-gather.15.cloned.1.call-done = bf16[2048,2816]{1,0:T(8,128)(2,1)} async-done(((bf16[128,2816]{1,0:T(8,128)(2,1)}), bf16[2048,2816]{1,0:T(8,128)(2,1)}) %all-gather.15.cloned.1.call-update) | async-done | bytes 11534352 | tf_op jit(solution)/shard_map/all_gather | solution.py:23
  367.6 7.7 %convolution_convert_fusion = bf16[256,2816]{1,0:T(8,128)(2,1)S(1)} fusion(bf16[256,2048]{1,0:T(8,128)(2,1)} %all-gather.11.cloned.1.call-done, bf16[2048,2816]{1,0:T(8,128)(2,1)} %all-gather.15.cloned.1.call-done), kind=kOutput, calls=%fused_computation.39 | convolution fusion | flops 2953510912 | bytes 14024704 | tf_op jit(solution)/shard_map/dot_general | solution.py:108
  375.4 86.6 %all-gather.13.cloned.1.call-done = bf16[2048,2816]{1,0:T(8,128)(2,1)} async-done(((bf16[128,2816]{1,0:T(8,128)(2,1)}), bf16[2048,2816]{1,0:T(8,128)(2,1)}) %all-gather.13.cloned.1.call-update) | async-done | bytes 11534352 | tf_op jit(solution)/shard_map/all_gather | solution.py:22
  462.0 7.7 %convolution_convert_fusion.1 = bf16[256,2816]{1,0:T(8,128)(2,1)S(1)} fusion(bf16[256,2048]{1,0:T(8,128)(2,1)} %all-gather.11.cloned.1.call-done, bf16[2048,2816]{1,0:T(8,128)(2,1)} %all-gather.13.cloned.1.call-done), kind=kOutput, calls=%fused_computation.40 | convolution fusion | flops 2953510912 | bytes 14024704 | tf_op jit(solution)/shard_map/dot_general | solution.py:107
  469.8 2.2 collective-permute-start
  472.0 1.2 slice_reduce_fusion.2
  473.2 0.8 maximum_convert_fusion
  474.0 3.3 fusion.22
  477.4 82.2 %all-gather.17.cloned.1.call-done = bf16[2816,2048]{1,0:T(8,128)(2,1)} async-done(((bf16[2816,128]{1,0:T(8,128)(2,1)}), bf16[2816,2048]{1,0:T(8,128)(2,1)}) %all-gather.17.cloned.1.call-update) | async-done | bytes 11534352 | tf_op jit(solution)/shard_map/all_gather | solution.py:25
  559.6 10.2 %convolution_convert_fusion.2 = bf16[256,2048]{1,0:T(8,128)(2,1)} fusion(bf16[2816,2048]{1,0:T(8,128)(2,1)} %all-gather.17.cloned.1.call-done, f32[256,5632]{1,0:T(8,128)} %fusion.22), kind=kOutput, calls=%fused_computation.44 | convolution fusion | flops 2957639680 | bytes 18350080 | tf_op jit(solution)/shard_map/dot_general | solution.py:122
  569.8 18.7 %reduce-scatter.2.cloned.1.call-done = bf16[128,2048]{1,0:T(8,128)(2,1)} async-done(((bf16[256,2048]{1,0:T(8,128)(2,1)}), bf16[128,2048]{1,0:T(8,128)(2,1)}) %reduce-scatter.2.cloned.1.call-update) | async-done | bytes 524304 | tf_op jit(solution)/shard_map/reduce_scatter | solution.py:121
  588.5 1.2 fusion.28
  589.7 2.1 fusion.33
  (53 shorter events, 5.2 us)
Async XLA Ops:
  6.5 176.1 %copy-start = (bf16[512,2048]{1,0:T(8,128)(2,1)S(1)}, bf16[512,2048]{1,0:T(8,128)(2,1)}, u32[]{:S(2)}) copy-start(bf16[512,2048]{1,0:T(8,128)(2,1)} %param.21) | copy-start | bytes 6291460
  6.5 93.7 %copy-start.7 = (f32[4]{0:T(128)S(1)}, f32[4]{0:T(128)}, u32[]{:S(2)}) copy-start(f32[4]{0:T(128)} %param.19) | copy-start | bytes 52
  6.5 47.2 %all-gather.7.cloned.1.call-start = ((), (), s32[]{:S(2)}) async-start(), calls=%async_computation.2 | async-start | bytes 2228224 | tf_op jit(solution)/shard_map/all_gather | solution.py:96
  7.3 88.8 %all-gather.9.cloned.1.call-start = ((), (), s32[]{:S(2)}) async-start(), calls=%async_computation.3 | async-start | bytes 2228224 | tf_op jit(solution)/shard_map/all_gather | solution.py:97
  8.0 263.5 %all-gather.11.cloned.1.call-start = ((), (), s32[]{:S(2)}) async-start(), calls=%async_computation.4 | async-start | bytes 1572864 | tf_op jit(solution)/shard_map/all_gather | solution.py:106
  100.2 82.9 %copy-start.8 = (f32[2048]{0:T(1024)S(1)}, f32[2048]{0:T(1024)}, u32[]{:S(2)}) copy-start(f32[2048]{0:T(1024)} %param.22) | copy-start | bytes 24580
  100.3 85.2 %copy-start.9 = (f32[2048]{0:T(1024)S(1)}, f32[2048]{0:T(1024)}, u32[]{:S(2)}) copy-start(f32[2048]{0:T(1024)} %param.23) | copy-start | bytes 24580
  137.4 3.2 copy-start.1
  150.3 15.1 %copy-start.2 = (bf16[4096,4,64]{0,2,1:T(8,128)(2,1)S(1)}, bf16[4096,4,64]{0,2,1:T(8,128)(2,1)}, u32[]{:S(2)}) copy-start(bf16[4096,4,64]{0,2,1:T(8,128)(2,1)} %get-tuple-element.219) | copy-start | bytes 6291460 | tf_op jit(solution)/shard_map/while
  175.5 12.7 %copy-start.5 = (f32[3,2816]{1,0:T(4,128)S(1)}, f32[3,2816]{1,0:T(4,128)}, u32[]{:S(2)}) copy-start(f32[3,2816]{1,0:T(4,128)} %param.26) | copy-start | bytes 101380
  175.5 13.4 %copy-start.6 = (f32[3,2816]{1,0:T(4,128)S(1)}, f32[3,2816]{1,0:T(4,128)}, u32[]{:S(2)}) copy-start(f32[3,2816]{1,0:T(4,128)} %param.27) | copy-start | bytes 101380
  184.6 0.8 copy-start.3
  186.4 181.2 %all-gather.15.cloned.1.call-start = ((), (), s32[]{:S(2)}) async-start(), calls=%async_computation.6 | async-start | bytes 12255232 | tf_op jit(solution)/shard_map/all_gather | solution.py:23
  187.0 275.0 %all-gather.13.cloned.1.call-start = ((), (), s32[]{:S(2)}) async-start(), calls=%async_computation.5 | async-start | bytes 12255232 | tf_op jit(solution)/shard_map/all_gather | solution.py:22
  187.6 372.0 %all-gather.17.cloned.1.call-start = ((), (), s32[]{:S(2)}) async-start(), calls=%async_computation.7 | async-start | bytes 12255232 | tf_op jit(solution)/shard_map/all_gather | solution.py:25
  188.2 400.3 %reduce-scatter.2.cloned.1.call-start = ((), (), s32[]{:S(2)}) async-start(), calls=%async_computation.8 | async-start | bytes 1572864 | tf_op jit(solution)/shard_map/reduce_scatter | solution.py:121
  469.8 3.4 collective-permute-start
  477.4 112.4 %copy-start.4 = (bf16[128,2048]{1,0:T(8,128)(2,1)S(1)}, bf16[128,2048]{1,0:T(8,128)(2,1)}, u32[]{:S(2)}) copy-start(bf16[128,2048]{1,0:T(8,128)(2,1)} %copy-done.3) | copy-start | bytes 1572868
  477.4 112.4 %copy-start.10 = (f32[2048]{0:T(1024)S(1)}, f32[2048]{0:T(1024)}, u32[]{:S(2)}) copy-start(f32[2048]{0:T(1024)} %param.29) | copy-start | bytes 24580
Sparse Core Ops, SparseCore 0:
  9.5 44.1 all-gather.6
  55.9 40.1 all-gather.8
  186.5 84.8 all-gather.10
  273.6 93.9 all-gather.14
  369.8 92.2 all-gather.12
  464.0 95.4 all-gather.16
  569.9 18.5 reduce-scatter.1
where the time goes:
time: 601 us; the launch traced here: 599 us
  waiting for transfers between devices  452 us (75%)
  other arithmetic  54.1 us (9%)
  matrix products  39.3 us (7%)
  local copies, waits for them, and re-layouts  20.9 us (3%)
  between operations  13.9 us (2%)
  loops' own time  9.61 us (2%)
  blocking collectives  7.01 us (1%)
    all_gather x1, waiting for transfers between devices, collect_weights(): lax.all_gather(w_up, 'sp', axis=0, tiled=True)  96.2 us
    all_gather x1, waiting for transfers between devices, collect_weights(): lax.all_gather(w_gate, 'sp', axis=0, tiled=True)  86.6 us
    all_gather x1, waiting for transfers between devices, collect_weights(): down_whole = lax.all_gather(w_down, 'sp', axis=1, tiled=True)  82.2 us
    all_gather x1, waiting for transfers between devices, local(): piece = lax.all_gather(normed, 'tp', axis=0, tiled=True)  82 us
    all_gather x1, waiting for transfers between devices, local(): lax.all_gather(keys, 'sp', axis=0, tiled=True)  44.6 us
    all_gather x1, waiting for transfers between devices, local(): lax.all_gather(values, 'sp', axis=0, tiled=True)  38.3 us
    another operation x2, other arithmetic  24.2 us
    reduce_scatter x1, waiting for transfers between devices, local(): lax.psum_scatter(jnp.dot(hidden, down_whole, preferred_element_type=jnp.f...  18.7 us
  transfers between devices with their start and end apart: 8, of which 7 were waited for; matrix products, arithmetic and copies ran while one was open for 5% of the time, Pallas kernels for 0%

commit v1 on v0

--- a/solution.py
+++ b/solution.py
@@ -1,6 +1,10 @@
+import functools
+
 import jax
 import jax.numpy as jnp
 from jax import lax
+from jax.experimental import pallas as pl
+from jax.experimental.pallas import tpu as pltpu
 from jax.sharding import PartitionSpec as P
 
 HEAD_DIM = 64
@@ -75,7 +79,7 @@
     return accum.transpose(1, 0, 2).reshape(tok_rows, local_heads * HEAD_DIM).astype(jnp.bfloat16)
 
 
-def local(
+def generic_local(
     queries,
     keys,
     values,
@@ -129,6 +133,348 @@
     )
 
 
+MESH = pl.DeviceIdType.MESH
+NZ, NY, NC = 4, 2, 2
+
+
+def front_kernel(
+    q_ref, k_ref, v_ref, shift_ref, wg_ref, wu_ref, wd_ref,
+    att_ref, gate_ref, up_ref, down_ref,
+    kbuf, vbuf, qs, acc, tail, tri, own_g, own_u, own_d,
+    kv_send, kv_recv, w_send, w_recv, loc_in, loc_out,
+):
+    rows, width = q_ref.shape
+    heads = width // HEAD_DIM
+    depth = wg_ref.shape[0]
+    units = gate_ref.shape[1]
+    cols = wd_ref.shape[1]
+    sp = lax.axis_index("sp")
+    z, y, c = sp // (NY * NC), (sp // NC) % NY, sp % NC
+    half = z // 2
+    inner = (z == 1) | (z == 2)
+    cross_in = 2 - half
+    cross_out = 3 - 3 * half
+    z_mate = z + 1 - 2 * lax.rem(z, 2)
+
+    def dev(zz, yy, cc):
+        return (zz * NY + yy) * NC + cc
+
+    y_dev, c_dev, m_dev = dev(z, 1 - y, c), dev(z, y, 1 - c), dev(z_mate, y, c)
+
+    def remote(src, dst, ssem, rsem, target):
+        return pltpu.make_async_remote_copy(
+            src_ref=src, dst_ref=dst, send_sem=ssem, recv_sem=rsem,
+            device_id={"sp": target}, device_id_type=MESH,
+        )
+
+    own = (own_g, own_u, own_d)
+    loads = [
+        pltpu.make_async_copy(src, dst, loc_in.at[i])
+        for i, (src, dst) in enumerate(zip((wg_ref, wu_ref, wd_ref), own))
+    ]
+    for copy in loads:
+        copy.start()
+
+    barrier = pltpu.get_barrier_semaphore()
+    for step in range(1, NZ):
+        pl.semaphore_signal(
+            barrier, inc=1, device_id={"sp": dev(lax.rem(z + step, NZ), y, c)}, device_id_type=MESH
+        )
+    for target in (y_dev, c_dev):
+        pl.semaphore_signal(barrier, inc=1, device_id={"sp": target}, device_id_type=MESH)
+    pl.semaphore_wait(barrier, NZ + 1)
+
+    def kv_slot(buf, shard):
+        return buf.at[pl.ds(pl.multiple_of(shard * rows, rows), rows), :]
+
+    def kv_copies(shard, first, kind, target):
+        out = []
+        for i, (src, buf) in enumerate(((k_ref, kbuf), (v_ref, vbuf))):
+            dst = kv_slot(buf, shard)
+            out.append(
+                remote(src if first else dst, dst, kv_send.at[i, kind, shard], kv_recv.at[i, shard], target)
+            )
+        return out
+
+    def own_part(a, part):
+        if a < 2:
+            return own[a].at[:, pl.ds(pl.multiple_of(part * units, 128), units)]
+        return own[a].at[pl.ds(pl.multiple_of(part * units, 128), units), :]
+
+    def slot(a, shard):
+        if a < 2:
+            return (gate_ref, up_ref)[a].at[pl.ds(pl.multiple_of(shard * depth, depth), depth), :]
+        return down_ref.at[:, pl.ds(pl.multiple_of(shard * cols, cols), cols)]
+
+    def w_copy(a, shard, kind, target, first=False, part=None):
+        dst = slot(a, shard)
+        src = own_part(a, half if part is None else part) if first else dst
+        return remote(src, dst, w_send.at[a, kind, shard], w_recv.at[a, shard], target)
+
+    for dz in range(1, NZ):
+        @pl.when(z + dz < NZ)
+        def _():
+            for copy in kv_copies(sp, True, dz - 1, dev(z + dz, y, c)):
+                copy.start()
+    for kind, target in ((3, y_dev), (4, c_dev)):
+        for copy in kv_copies(sp, True, kind, target):
+            copy.start()
+
+    for a in range(3):
+        loads[a].wait()
+        w_copy(a, sp, 0, dev(cross_in, y, c), True, 1 - half).start()
+    for a in range(3):
+        w_copy(a, sp, 1, m_dev, True).start()
+        w_copy(a, sp, 3, c_dev, True).start()
+    stores = [
+        pltpu.make_async_copy(own_part(a, half), slot(a, sp), loc_out.at[a]) for a in range(3)
+    ]
+    for copy in stores:
+        copy.start()
+
+    lane_head = lax.broadcasted_iota(jnp.int32, (rows, width), 1) // HEAD_DIM
+    q_all = q_ref[...].astype(jnp.float32) * HEAD_DIM ** (-0.5)
+    for h in range(heads):
+        qs[h] = jnp.where(lane_head == h, q_all, 0.0).astype(jnp.bfloat16)
+    r_idx = lax.broadcasted_iota(jnp.int32, (rows, rows), 0)
+    c_idx = lax.broadcasted_iota(jnp.int32, (rows, rows), 1)
+    tri[...] = jnp.where(r_idx > c_idx, 1.0, 0.0).astype(jnp.bfloat16)
+    acc[...] = jnp.zeros_like(acc)
+    tail[...] = jnp.zeros_like(tail)
+
+    def attend(kb, vb, masked):
+        for h in range(heads):
+            scores = lax.dot_general(
+                qs[h], kb, (((1,), (1,)), ((), ())), preferred_element_type=jnp.float32
+            ) - shift_ref[h]
+            keep = -(jnp.maximum(scores, 0.0) + jnp.log(1.0 + jnp.exp(-jnp.abs(scores))))
+            take = scores + keep
+            if masked:
+                keep = jnp.where(c_idx < r_idx, keep, 0.0)
+            high = keep.astype(jnp.bfloat16)
+            low = (keep - high.astype(jnp.float32)).astype(jnp.bfloat16)
+            later = jnp.dot(high, tri[...], preferred_element_type=jnp.float32) + jnp.dot(
+                low, tri[...], preferred_element_type=jnp.float32
+            )
+            before = tail[h]
+            weights = jnp.exp(take + later + before[:, 0:1])
+            if masked:
+                weights = jnp.where(c_idx < r_idx, weights, 0.0)
+            acc[h] += jnp.dot(weights.astype(jnp.bfloat16), vb, preferred_element_type=jnp.float32)
+            tail[h] = before + (later[:, 0:1] + keep[:, 0:1])
+
+    attend(k_ref[...], v_ref[...], True)
+
+    for dz in range(1, NZ):
+        @pl.when(z >= dz)
+        def _():
+            shard = dev(z - dz, y, c)
+            for copy in kv_copies(shard, False, 3, y_dev):
+                copy.wait_recv()
+                copy.start()
+            for copy in kv_copies(shard, False, 4, c_dev):
+                copy.start()
+    for a in range(3):
+        w_copy(a, sp, 2, y_dev, True).start()
+    for dz in range(NZ):
+        @pl.when(z >= dz)
+        def _():
+            shard = dev(z - dz, 1 - y, c)
+            for copy in kv_copies(shard, False, 4, c_dev):
+                copy.wait_recv()
+                copy.start()
+    for dz in range(NZ):
+        @pl.when(z >= dz)
+        def _():
+            for yy in (0, 1):
+                for copy in kv_copies(dev(z - dz, yy, 1 - c), False, 4, c_dev):
+                    copy.wait_recv()
+
+    def blocks(first, last):
+        def body(i, carry):
+            shard = sp - i
+            attend(kv_slot(kbuf, shard)[...], kv_slot(vbuf, shard)[...], False)
+            return carry
+
+        lax.fori_loop(jnp.minimum(first, sp + 1), jnp.minimum(last, sp + 1), body, 0)
+
+    def arrived(zz, to_mate):
+        shard = dev(zz, y, c)
+        for a in range(3):
+            w_copy(a, shard, 1, m_dev).wait_recv()
+            if to_mate:
+                w_copy(a, shard, 1, m_dev).start()
+            w_copy(a, shard, 2, y_dev).start()
+            w_copy(a, shard, 3, c_dev).start()
+
+    blocks(1, 3)
+    @pl.when(inner)
+    def _():
+        arrived(cross_in, True)
+    blocks(3, 6)
+    arrived(z_mate, False)
+    blocks(6, 9)
+    @pl.when(inner)
+    def _():
+        arrived(cross_out, True)
+    blocks(9, NZ * NY * NC)
+
+    total = jnp.zeros((rows, width), jnp.float32)
+    for h in range(heads):
+        total = jnp.where(lane_head == h, acc[h], total)
+    att_ref[...] = total.astype(jnp.bfloat16)
+
+    @pl.when(jnp.logical_not(inner))
+    def _():
+        arrived(cross_in, False)
+        arrived(cross_out, False)
+    for zz in (z, z_mate, cross_in, cross_out):
+        for a in range(3):
+            copy = w_copy(a, dev(zz, 1 - y, c), 3, c_dev)
+            copy.wait_recv()
+            copy.start()
+    for zz in (z, z_mate, cross_in, cross_out):
+        for yy in (y, 1 - y):
+            for a in range(3):
+                w_copy(a, dev(zz, yy, 1 - c), 3, c_dev).wait_recv()
+
+    for copy in stores:
+        copy.wait()
+    for dz in range(1, NZ):
+        @pl.when(z + dz < NZ)
+        def _():
+            for copy in kv_copies(sp, True, dz - 1, dev(z + dz, y, c)):
+                copy.wait_send()
+    for dz in range(NZ):
+        @pl.when(z >= dz)
+        def _():
+            for copy in kv_copies(dev(z - dz, y, c), False, 3, y_dev):
+                copy.wait_send()
+            for yy in (y, 1 - y):
+                for copy in kv_copies(dev(z - dz, yy, c), False, 4, c_dev):
+                    copy.wait_send()
+    for a in range(3):
+        w_copy(a, sp, 0, m_dev).wait_send()
+        w_copy(a, sp, 1, m_dev).wait_send()
+        for zz in (z, z_mate, cross_in, cross_out):
+            w_copy(a, dev(zz, y, c), 2, y_dev).wait_send()
+            for yy in (y, 1 - y):
+                w_copy(a, dev(zz, yy, c), 3, c_dev).wait_send()
+
+    @pl.when(inner)
+    def _():
+        for zz in (cross_in, cross_out):
+            for a in range(3):
+                w_copy(a, dev(zz, y, c), 1, m_dev).wait_send()
+
+
+def front(queries, keys, values, score_shift, w_gate, w_up, w_down):
+    shards = lax.axis_size("sp")
+    rows, width = queries.shape
+    heads = width // HEAD_DIM
+    depth, units = w_gate.shape[0], w_gate.shape[1] // 2
+    cols = w_down.shape[1]
+    vmem = pl.BlockSpec(memory_space=pltpu.VMEM)
+    hbm = pl.BlockSpec(memory_space=pl.ANY)
+    return pl.pallas_call(
+        front_kernel,
+        out_shape=(
+            jax.ShapeDtypeStruct((rows, width), jnp.bfloat16),
+            jax.ShapeDtypeStruct((shards * depth, units), jnp.bfloat16),
+            jax.ShapeDtypeStruct((shards * depth, units), jnp.bfloat16),
+            jax.ShapeDtypeStruct((units, shards * cols), jnp.bfloat16),
+        ),
+        in_specs=[vmem, vmem, vmem, pl.BlockSpec(memory_space=pltpu.SMEM), hbm, hbm, hbm],
+        out_specs=(vmem, hbm, hbm, hbm),
+        scratch_shapes=[
+            pltpu.VMEM((shards * rows, width), jnp.bfloat16),
+            pltpu.VMEM((shards * rows, width), jnp.bfloat16),
+            pltpu.VMEM((heads, rows, width), jnp.bfloat16),
+            pltpu.VMEM((heads, rows, width), jnp.float32),
+            pltpu.VMEM((heads, rows, 128), jnp.float32),
+            pltpu.VMEM((rows, rows), jnp.bfloat16),
+            pltpu.VMEM(w_gate.shape, jnp.bfloat16),
+            pltpu.VMEM(w_up.shape, jnp.bfloat16),
+            pltpu.VMEM(w_down.shape, jnp.bfloat16),
+            pltpu.SemaphoreType.DMA((2, 5, shards)),
+            pltpu.SemaphoreType.DMA((2, shards)),
+            pltpu.SemaphoreType.DMA((3, 4, shards)),
+            pltpu.SemaphoreType.DMA((3, shards)),
+            pltpu.SemaphoreType.DMA((3,)),
+            pltpu.SemaphoreType.DMA((3,)),
+        ],
+        compiler_params=pltpu.CompilerParams(collective_id=0, has_side_effects=True),
+        name="front",
+    )(queries, keys, values, score_shift, w_gate, w_up, w_down)
+
+
+def local(
+    queries, keys, values, score_shift, resid, w_out, gain_mix, gain_pre,
+    w_gate, w_up, conv_gate, conv_up, w_down, gain_post,
+):
+    attended, gate_w, up_w, down_w = front(
+        queries, keys, values, score_shift, w_gate, w_up, w_down
+    )
+    shards = lax.axis_size("sp")
+    hop = shards // 2
+    sp = lax.axis_index("sp")
+    half = sp // hop
+    units = gate_w.shape[1]
+    pairs = [(i, (i + hop) % shards) for i in range(shards)]
+    head_rows = lax.all_to_all(attended, "tp", split_axis=0, concat_axis=1, tiled=True)
+    mixed = jnp.dot(head_rows, w_out, preferred_element_type=jnp.float32).astype(jnp.bfloat16)
+    middle = (resid.astype(jnp.float32) + gain_mix * rms_scale(mixed.astype(jnp.float32))).astype(
+        jnp.bfloat16
+    )
+    normed = (gain_pre * rms_scale(middle.astype(jnp.float32))).astype(jnp.bfloat16)
+    piece = lax.all_gather(normed, "tp", axis=0, tiled=True)
+    other = lax.ppermute(piece, "sp", pairs)
+    run = piece.shape[0]
+    tokens = jnp.where(
+        half == 0, jnp.concatenate([piece, other], 0), jnp.concatenate([other, piece], 0)
+    )
+    conv_g = lax.dynamic_slice_in_dim(conv_gate, half * units, units, 1)
+    conv_u = lax.dynamic_slice_in_dim(conv_up, half * units, units, 1)
+    gate_part = jnp.dot(tokens, gate_w, preferred_element_type=jnp.float32).astype(jnp.bfloat16)
+    up_part = jnp.dot(tokens, up_w, preferred_element_type=jnp.float32).astype(jnp.bfloat16)
+    last = KERNEL - 1
+    edges = jnp.stack(
+        [
+            jnp.stack([part[run - last : run], part[2 * run - last :]])
+            for part in (gate_part, up_part)
+        ]
+    )
+    ring = [(i, i // hop * hop + (i + 1) % hop) for i in range(shards)]
+    before = lax.ppermute(edges, "sp", ring)
+    first = sp % hop == 0
+    before = jnp.where(
+        first, jnp.stack([jnp.zeros_like(before[:, 0]), before[:, 0]], axis=1), before
+    )
+
+    def convolve(part, edge, taps):
+        out = []
+        for r in range(2):
+            ext = jnp.concatenate([edge[r], part[r * run : (r + 1) * run]], 0).astype(jnp.float32)
+            total = taps[0] * ext[0:run]
+            for tap in range(1, KERNEL):
+                total = total + taps[tap] * ext[tap : tap + run]
+            out.append(total)
+        return jnp.concatenate(out, 0)
+
+    hidden = (
+        jax.nn.silu(convolve(gate_part, before[0], conv_g)) * convolve(up_part, before[1], conv_u)
+    ).astype(jnp.bfloat16)
+    partial = jnp.dot(hidden, down_w, preferred_element_type=jnp.float32).astype(jnp.bfloat16)
+    away = lax.dynamic_slice_in_dim(partial, (1 - half) * run, run, 0)
+    mine = lax.dynamic_slice_in_dim(partial, half * run, run, 0)
+    back = lax.ppermute(away, "sp", pairs)
+    both = (mine.astype(jnp.float32) + back.astype(jnp.float32)).astype(jnp.bfloat16)
+    summed = lax.psum_scatter(both, "tp", scatter_dimension=0, tiled=True)
+    return (middle.astype(jnp.float32) + gain_post * rms_scale(summed.astype(jnp.float32))).astype(
+        jnp.bfloat16
+    )
+
+
 def solution(mesh):
     in_specs = (
         P("sp", "tp"),
@@ -147,4 +493,5 @@
         P(),
     )
     out_specs = P(("sp", "tp"), None)
-    return jax.shard_map(local, mesh=mesh, in_specs=in_specs, out_specs=out_specs, check_vma=False)
+    split = mesh.shape["sp"] == NZ * NY * NC and mesh.shape["tp"] == 2
+    return jax.shard_map(local if split else generic_local, mesh=mesh, in_specs=in_specs, out_specs=out_specs, check_vma=False)

time: 601 us -> 359 us (0.60)
  waiting for transfers between devices: 452 us -> 180 us
  Pallas kernels: 0 us -> 116 us
  other arithmetic: 54.1 us -> 10 us
  matrix products: 39.3 us -> 19.1 us
  local copies, waits for them, and re-layouts: 20.9 us -> 7.71 us
  loops' own time: 9.61 us -> 0 us
    all_gather x5 -> x0, waiting for transfers between devices: 348 us -> none  [the longest x1 96.2 us: collect_weights(): lax.all_gather(w_up, 'sp', axis=0, tiled=True)]
    pallas_call x0 -> x1, Pallas kernels: none -> 116 us  [front(): pl.pallas_call(front_kernel, out_shape=(jax.ShapeDtypeStruct((rows, width...]
    ppermute x1 -> x3, waiting for transfers between devices: 0.01 us -> 94.4 us  [the longest x1 45.4 us: local(): back = lax.ppermute(away, 'sp', pairs)]
    another operation x3, other arithmetic: 28.7 us -> 0.08 us  [local(): jnp.stack([jnp.stack([part[run - last:run], part[2 * run - last:]]) for p...]
    dot_general x5 -> x3, matrix products: 38.8 us -> 18.5 us  [the longest x1 7.4 us: local(): jnp.dot(tokens, gate_w, preferred_element_type=jnp.float32)]
    all_gather x1, waiting for transfers between devices: 82 us -> 66.6 us  [local(): piece = lax.all_gather(normed, 'tp', axis=0, tiled=True)]
    convert_element_type x3, other arithmetic: 15.9 us -> 3.52 us  [the longest x1 2.92 us: local(): (mine.astype(jnp.float32) + back.astype(jnp.float32)).astype(jnp.bfloat16)]
    another operation x1 -> x0, loops' own time: 9.61 us -> none  [stick_attention(): accum, _ = lax.fori_loop(0, last_block + 1, visit, start_carry)]
  transfers between devices with their start and end apart: 8 -> 5, of which waited for: 7 -> 5; matrix products, arithmetic and copies ran while one was open for 5% -> 0% of each run, Pallas kernels for 0% -> 0%
where the time goes in v1:
time: 359 us; the launch traced here: 358 us
  waiting for transfers between devices  180 us (50%)
  Pallas kernels  116 us (32%)
  matrix products  19.1 us (5%)
  between operations  13.6 us (4%)
  other arithmetic  10 us (3%)
  local copies, waits for them, and re-layouts  7.71 us (2%)
  blocking collectives  7.06 us (2%)
  starting transfers between devices  4.45 us (1%)
    pallas_call x1, Pallas kernels, front(): pl.pallas_call(front_kernel, out_shape=(jax.ShapeDtypeStruct((rows, width...  116 us
    all_gather x1, waiting for transfers between devices, local(): piece = lax.all_gather(normed, 'tp', axis=0, tiled=True)  66.6 us
    ppermute x1, waiting for transfers between devices, local(): back = lax.ppermute(away, 'sp', pairs)  45.4 us
    ppermute x1, waiting for transfers between devices, local(): other = lax.ppermute(piece, 'sp', pairs)  45 us
    reduce_scatter x1, waiting for transfers between devices, local(): summed = lax.psum_scatter(both, 'tp', scatter_dimension=0, tiled=True)  19.2 us
    dot_general x1, matrix products, local(): jnp.dot(tokens, gate_w, preferred_element_type=jnp.float32)  7.4 us
  transfers between devices with their start and end apart: 5, of which 5 were waited for; matrix products, arithmetic and copies ran while one was open for 0% of the time, Pallas kernels for 0%

profile of v1, /device:TPU:0, one launch (start us, length us, event | category | flops | bytes accessed | tf_op | source)
XLA Modules:
  0.0 358.1 jit_solution(16857917446685707047)
XLA Ops:
  6.5 115.9 %front.1 = (bf16[256,256]{1,0:T(8,128)(2,1)}, bf16[2048,1408]{1,0:T(8,128)(2,1)}, bf16[2048,1408]{1,0:T(8,128)(2,1)}, bf16[1408,2048]{1,0:T(8,128)(2,1)}) custom-call(bf16[256,256]{1,0:T(8,128)(2,1)} %q_ref.1, bf16[256,256]{1,0:T(8,128)(2,1)} %k_ref.1, bf16[256,256]{1,0:T(8,128)(2,1)} %v_ref.1, f32[4]{0:T(128)} %shift_ref.1, bf16[128,2816]{1,0:T(8,128)(2,1)} %wg_ref.1, ...), custom_call_target="tpu_custom_call" | custom-call | tf_op jit(solution)/shard_map/front/pallas_call | solution.py:379
  122.5 1.0 copy.15
  123.5 7.1 %all_to_all.19 = bf16[2,128,256]{1,2,0:T(8,128)(2,1)S(1)} all-to-all(bf16[2,128,256]{1,2,0:T(8,128)(2,1)S(1)} %copy.15), channel_id=1, replica_groups=mesh['sp'=16,'tp'=2] {'tp'}, dimensions={0} | all-to-all | bytes 262144 | tf_op jit(solution)/shard_map/all_to_all | solution.py:424
  130.6 0.6 multiply_reduce_fusion
  131.1 0.5 copy-done.2
  131.6 0.4 fusion.14
  132.0 1.0 fusion.16
  133.0 0.2 reduce-scatter.2.cloned.1.call-start
  133.2 66.6 %all-gather.2.cloned.1.call-done = bf16[256,2048]{1,0:T(8,128)(2,1)} async-done(((bf16[128,2048]{1,0:T(8,128)(2,1)}), bf16[256,2048]{1,0:T(8,128)(2,1)}) %all-gather.2.cloned.1.call-update) | async-done | bytes 1048592 | tf_op jit(solution)/shard_map/all_gather | solution.py:430
  199.8 2.4 collective-permute-start
  202.2 1.0 dynamic-slice_reduce_fusion.2
  203.2 45.0 %collective-permute-done = bf16[256,2048]{1,0:T(8,128)(2,1)} collective-permute-done((bf16[256,2048]{1,0:T(8,128)(2,1)}, bf16[256,2048]{1,0:T(8,128)(2,1)}, u32[]{:S(2)}, u32[]{:S(2)}) %collective-permute-start) | collective-permute-done | bytes 1048608 | tf_op jit(solution)/shard_map/ppermute | solution.py:431
  248.2 7.4 %convolution_convert_fusion.1 = bf16[512,1408]{1,0:T(8,128)(2,1)S(1)} fusion(bf16[2048,1408]{1,0:T(8,128)(2,1)} %get-tuple-element.10, bf16[256,2048]{1,0:T(8,128)(2,1)} %collective-permute-done, bf16[256,2048]{1,0:T(8,128)(2,1)} %all-gather.2.cloned.1.call-done, pred[]{:T(512)S(6)} %eq.9), kind=kOutput, calls=%fused_computation.1 | convolution fusion | flops 2962948096 | bytes 9306113 | tf_op jit(solution)/shard_map/dot_general | solution.py:438
  255.6 0.1 fusion.22
  255.8 1.1 copy-done.6
  256.9 6.8 %convolution_convert_fusion = bf16[512,1408]{1,0:T(8,128)(2,1)S(1)} fusion(bf16[2048,1408]{1,0:T(8,128)(2,1)} %get-tuple-element.11, bf16[256,2048]{1,0:T(8,128)(2,1)} %collective-permute-done, bf16[256,2048]{1,0:T(8,128)(2,1)S(1)} %copy-done.6, pred[]{:T(512)S(6)} %eq.9), kind=kOutput, calls=%fused_computation | convolution fusion | flops 2962948096 | bytes 9306113 | tf_op jit(solution)/shard_map/dot_general | solution.py:439
  263.8 0.1 fusion.23
  263.9 4.0 %collective-permute-done.1 = bf16[2,2,2,1408]{3,2,1,0:T(2,128)(2,1)S(1)} collective-permute-done((bf16[2,2,2,1408]{3,2,1,0:T(2,128)(2,1)S(1)}, bf16[2,2,2,1408]{3,2,1,0:T(2,128)(2,1)S(1)}, u32[]{:S(2)}, u32[]{:S(2)}) %collective-permute-start.1) | collective-permute-done | bytes 22560 | tf_op jit(solution)/shard_map/ppermute | solution.py:448
  268.0 0.3 maximum_convert_fusion
  268.3 0.3 maximum_convert_fusion.2
  268.6 0.8 fusion.9
  269.5 0.8 fusion.5
  270.4 1.4 slice-done.1
  271.8 4.3 %convolution_convert_fusion.2 = bf16[512,2048]{1,0:T(8,128)(2,1)S(1)} fusion(bf16[1408,2048]{1,0:T(8,128)(2,1)S(1)} %bitcast.32, f32[256,1408]{1,0:T(8,128)S(1)} %get-tuple-element.32, f32[256,1408]{1,0:T(8,128)S(1)} %get-tuple-element.31, f32[256,1408]{1,0:T(8,128)S(1)} %get-tuple-element.30, f32[256,1408]{1,0:T(8,128)S(1)} %get-tuple-element.29), kind=kOutput, calls=%fused_computation.2 | convolution fusion | flops 2959605760 | bytes 13631488 | tf_op jit(solution)/shard_map/dot_general | solution.py:467
  276.2 1.3 copy-done.1
  277.5 1.1 constant_dynamic-slice_fusion
  278.6 1.8 collective-permute-start.2
  280.3 45.4 %collective-permute-done.2 = bf16[256,2048]{1,0:T(8,128)(2,1)} collective-permute-done((bf16[256,2048]{1,0:T(8,128)(2,1)}, bf16[256,2048]{1,0:T(8,128)(2,1)}, u32[]{:S(2)}, u32[]{:S(2)}) %collective-permute-start.2) | collective-permute-done | bytes 1048608 | tf_op jit(solution)/shard_map/ppermute | solution.py:470
  325.7 2.9 add_convert_fusion
  328.7 19.2 %reduce-scatter.2.cloned.1.call-done = bf16[128,2048]{1,0:T(8,128)(2,1)} async-done(((bf16[256,2048]{1,0:T(8,128)(2,1)}), bf16[128,2048]{1,0:T(8,128)(2,1)}) %reduce-scatter.2.cloned.1.call-update) | async-done | bytes 524304 | tf_op jit(solution)/shard_map/reduce_scatter | solution.py:472
  347.9 1.2 fusion.12
  349.1 2.1 fusion.17
  (30 shorter events, 0.3 us)
Async XLA Ops:
  6.5 124.0 %copy-start = (bf16[512,2048]{1,0:T(8,128)(2,1)S(1)}, bf16[512,2048]{1,0:T(8,128)(2,1)}, u32[]{:S(2)}) copy-start(bf16[512,2048]{1,0:T(8,128)(2,1)} %param.19) | copy-start | bytes 6291460
  6.5 193.3 %all-gather.2.cloned.1.call-start = ((), (), s32[]{:S(2)}) async-start(), calls=%async_computation.2 | async-start | bytes 1572864 | tf_op jit(solution)/shard_map/all_gather | solution.py:430
  130.5 1.0 copy-start.2
  130.5 1.0 copy-start.3
  131.1 0.9 copy-start.4
  133.0 214.9 %reduce-scatter.2.cloned.1.call-start = ((), (), s32[]{:S(2)}) async-start(), calls=%async_computation.3 | async-start | bytes 1572864 | tf_op jit(solution)/shard_map/reduce_scatter | solution.py:472
  199.8 48.4 %collective-permute-start = (bf16[256,2048]{1,0:T(8,128)(2,1)}, bf16[256,2048]{1,0:T(8,128)(2,1)}, u32[]{:S(2)}, u32[]{:S(2)}) collective-permute-start(bf16[256,2048]{1,0:T(8,128)(2,1)} %all-gather.2.cloned.1.call-done), channel_id=1, source_target_pairs={{0,16},{2,18},{4,20},{6,22},{8,24},{10,26},{12,28},{14,30},{16,0},... | collective-permute-start | bytes 3145736 | tf_op jit(solution)/shard_map/ppermute | solution.py:431
  255.6 1.2 copy-start.6
  263.8 4.2 %collective-permute-start.1 = (bf16[2,2,2,1408]{3,2,1,0:T(2,128)(2,1)S(1)}, bf16[2,2,2,1408]{3,2,1,0:T(2,128)(2,1)S(1)}, u32[]{:S(2)}, u32[]{:S(2)}) collective-permute-start(bf16[2,2,2,1408]{3,2,1,0:T(2,128)(2,1)S(1)} %pad_maximum_fusion.1), channel_id=1, source_target_pairs={{0,2},{2,4},{4,6},{6,8},{8,10},{10,12},{12,14},{14,0},{16,18},{18,... | collective-permute-start | bytes 67592 | tf_op jit(solution)/shard_map/ppermute | solution.py:448
  268.6 1.7 slice-start
  269.5 2.3 slice-start.1
  276.1 1.3 copy-start.1
  278.6 47.1 %collective-permute-start.2 = (bf16[256,2048]{1,0:T(8,128)(2,1)}, bf16[256,2048]{1,0:T(8,128)(2,1)}, u32[]{:S(2)}, u32[]{:S(2)}) collective-permute-start(bf16[256,2048]{1,0:T(8,128)(2,1)} %constant_dynamic-slice_fusion), channel_id=1, source_target_pairs={{0,16},{2,18},{4,20},{6,22},{8,24},{10,26},{12,28},{14,30},{16,0},... | collective-permute-start | bytes 3145736 | tf_op jit(solution)/shard_map/ppermute | solution.py:470
  328.6 20.5 %copy-start.5 = (f32[2048]{0:T(1024)S(1)}, f32[2048]{0:T(1024)}, u32[]{:S(2)}) copy-start(f32[2048]{0:T(1024)} %param.27) | copy-start | bytes 24580
Sparse Core Ops, SparseCore 0:
  133.1 66.6 all-gather.1
  328.8 19.0 reduce-scatter.1

commit v2 on v1

--- a/solution.py
+++ b/solution.py
@@ -138,10 +138,10 @@
 
 
 def front_kernel(
-    q_ref, k_ref, v_ref, shift_ref, wg_ref, wu_ref, wd_ref,
-    att_ref, gate_ref, up_ref, down_ref,
-    kbuf, vbuf, qs, acc, tail, tri, own_g, own_u, own_d,
-    kv_send, kv_recv, w_send, w_recv, loc_in, loc_out,
+    q_ref, k_ref, v_ref, shift_ref, resid_ref, wo_ref, mix_ref, pre_ref, wg_ref, wu_ref, wd_ref,
+    mid_ref, tok_ref, gate_ref, up_ref, down_ref,
+    kbuf, vbuf, qs, acc, tail, tri, own_g, own_u, own_d, att, heads_in, mixed, normed,
+    kv_send, kv_recv, w_send, w_recv, loc_in, loc_out, x_sem, t_send, t_recv,
 ):
     rows, width = q_ref.shape
     heads = width // HEAD_DIM
@@ -182,7 +182,9 @@
         )
     for target in (y_dev, c_dev):
         pl.semaphore_signal(barrier, inc=1, device_id={"sp": target}, device_id_type=MESH)
-    pl.semaphore_wait(barrier, NZ + 1)
+    tp = lax.axis_index("tp")
+    pl.semaphore_signal(barrier, inc=1, device_id={"tp": 1 - tp}, device_id_type=MESH)
+    pl.semaphore_wait(barrier, NZ + 2)
 
     def kv_slot(buf, shard):
         return buf.at[pl.ds(pl.multiple_of(shard * rows, rows), rows), :]
@@ -274,21 +276,21 @@
                 copy.start()
             for copy in kv_copies(shard, False, 4, c_dev):
                 copy.start()
-    for a in range(3):
-        w_copy(a, sp, 2, y_dev, True).start()
-    for dz in range(NZ):
-        @pl.when(z >= dz)
-        def _():
-            shard = dev(z - dz, 1 - y, c)
-            for copy in kv_copies(shard, False, 4, c_dev):
+        w_copy(dz - 1, sp, 2, y_dev, True).start()
+
+    def plane(dz):
+        for copy in kv_copies(dev(z - dz, 1 - y, c), False, 4, c_dev):
+            copy.wait_recv()
+            copy.start()
+        for yy in (0, 1):
+            for copy in kv_copies(dev(z - dz, yy, 1 - c), False, 4, c_dev):
                 copy.wait_recv()
-                copy.start()
-    for dz in range(NZ):
-        @pl.when(z >= dz)
-        def _():
-            for yy in (0, 1):
-                for copy in kv_copies(dev(z - dz, yy, 1 - c), False, 4, c_dev):
-                    copy.wait_recv()
+        in_plane = lax.rem(sp, NY * NC)
+        if dz == 0:
+            blocks(1, in_plane + 1)
+        else:
+            base = in_plane + (dz - 1) * NY * NC + 1
+            blocks(base, base + NY * NC)
 
     def blocks(first, last):
         def body(i, carry):
@@ -296,7 +298,7 @@
             attend(kv_slot(kbuf, shard)[...], kv_slot(vbuf, shard)[...], False)
             return carry
 
-        lax.fori_loop(jnp.minimum(first, sp + 1), jnp.minimum(last, sp + 1), body, 0)
+        lax.fori_loop(first, last, body, 0)
 
     def arrived(zz, to_mate):
         shard = dev(zz, y, c)
@@ -307,26 +309,94 @@
             w_copy(a, shard, 2, y_dev).start()
             w_copy(a, shard, 3, c_dev).start()
 
-    blocks(1, 3)
+    plane(0)
     @pl.when(inner)
     def _():
         arrived(cross_in, True)
-    blocks(3, 6)
+    @pl.when(z >= 1)
+    def _():
+        plane(1)
     arrived(z_mate, False)
-    blocks(6, 9)
+    @pl.when(z >= 2)
+    def _():
+        plane(2)
     @pl.when(inner)
     def _():
         arrived(cross_out, True)
-    blocks(9, NZ * NY * NC)
+    @pl.when(z >= 3)
+    def _():
+        plane(3)
 
     total = jnp.zeros((rows, width), jnp.float32)
     for h in range(heads):
         total = jnp.where(lane_head == h, acc[h], total)
-    att_ref[...] = total.astype(jnp.bfloat16)
+    att[...] = total.astype(jnp.bfloat16)
+
+    own_rows = rows // 2
+    there = pl.ds(pl.multiple_of((1 - tp) * own_rows, own_rows), own_rows)
+    here = pl.ds(pl.multiple_of(tp * own_rows, own_rows), own_rows)
+    swap = pltpu.make_async_remote_copy(
+        src_ref=att.at[there, :], dst_ref=heads_in, send_sem=x_sem.at[0], recv_sem=x_sem.at[1],
+        device_id={"tp": 1 - tp}, device_id_type=MESH,
+    )
+    swap.start()
 
     @pl.when(jnp.logical_not(inner))
     def _():
         arrived(cross_in, False)
+
+    out_rows = pl.ds(pl.multiple_of(tp * width, width), width)
+    in_rows = pl.ds(pl.multiple_of((1 - tp) * width, width), width)
+    wide = mixed.shape[1]
+    step_cols = wide // 4
+    for n in range(4):
+        part = pl.ds(n * step_cols, step_cols)
+        mixed[:, part] = jnp.dot(
+            att[here, :], wo_ref[out_rows, part], preferred_element_type=jnp.float32
+        )
+    swap.wait_recv()
+    for n in range(4):
+        part = pl.ds(n * step_cols, step_cols)
+        mixed[:, part] += jnp.dot(
+            heads_in[...], wo_ref[in_rows, part], preferred_element_type=jnp.float32
+        )
+
+    @pl.loop(0, own_rows // 16)
+    def _(i):
+        part = pl.ds(pl.multiple_of(i * 16, 16), 16)
+        value = mixed[part, :].astype(jnp.bfloat16).astype(jnp.float32)
+        middle = (resid_ref[part, :].astype(jnp.float32) + mix_ref[...] * rms_scale(value)).astype(
+            jnp.bfloat16
+        )
+        mid_ref[part, :] = middle
+        normed[part, :] = (pre_ref[...] * rms_scale(middle.astype(jnp.float32))).astype(
+            jnp.bfloat16
+        )
+
+    p_dev = dev(lax.rem(z + 2, NZ), y, c)
+
+    def tok_slot(part, xx):
+        first = (part * 2 + xx) * own_rows
+        return tok_ref.at[pl.ds(pl.multiple_of(first, own_rows), own_rows), :]
+
+    def tok_copy(src, part, xx, kind, target):
+        return pltpu.make_async_remote_copy(
+            src_ref=src, dst_ref=tok_slot(part, xx), send_sem=t_send.at[kind],
+            recv_sem=t_recv.at[part, xx], device_id=target, device_id_type=MESH,
+        )
+
+    to_x = tok_copy(normed, half, tp, 0, {"tp": 1 - tp})
+    to_p = tok_copy(normed, half, tp, 1, {"sp": p_dev})
+    to_x.start()
+    to_p.start()
+    keep_own = pltpu.make_async_copy(normed, tok_slot(half, tp), x_sem.at[2])
+    keep_own.start()
+    relay = tok_copy(tok_slot(half, 1 - tp), half, 1 - tp, 2, {"sp": p_dev})
+    relay.wait_recv()
+    relay.start()
+
+    @pl.when(jnp.logical_not(inner))
+    def _():
         arrived(cross_out, False)
     for zz in (z, z_mate, cross_in, cross_out):
         for a in range(3):
@@ -338,6 +408,12 @@
             for a in range(3):
                 w_copy(a, dev(zz, yy, 1 - c), 3, c_dev).wait_recv()
 
+    for xx in (tp, 1 - tp):
+        tok_copy(normed, 1 - half, xx, 1, {"sp": p_dev}).wait_recv()
+
+    for copy in (swap, to_x, to_p, relay):
+        copy.wait_send()
+    keep_own.wait()
     for copy in stores:
         copy.wait()
     for dz in range(1, NZ):
@@ -368,7 +444,9 @@
                 w_copy(a, dev(zz, y, c), 1, m_dev).wait_send()
 
 
-def front(queries, keys, values, score_shift, w_gate, w_up, w_down):
+def front(
+    queries, keys, values, score_shift, resid, w_out, gain_mix, gain_pre, w_gate, w_up, w_down
+):
     shards = lax.axis_size("sp")
     rows, width = queries.shape
     heads = width // HEAD_DIM
@@ -379,13 +457,14 @@
     return pl.pallas_call(
         front_kernel,
         out_shape=(
-            jax.ShapeDtypeStruct((rows, width), jnp.bfloat16),
+            jax.ShapeDtypeStruct(resid.shape, jnp.bfloat16),
+            jax.ShapeDtypeStruct((4 * resid.shape[0], resid.shape[1]), jnp.bfloat16),
             jax.ShapeDtypeStruct((shards * depth, units), jnp.bfloat16),
             jax.ShapeDtypeStruct((shards * depth, units), jnp.bfloat16),
             jax.ShapeDtypeStruct((units, shards * cols), jnp.bfloat16),
         ),
-        in_specs=[vmem, vmem, vmem, pl.BlockSpec(memory_space=pltpu.SMEM), hbm, hbm, hbm],
-        out_specs=(vmem, hbm, hbm, hbm),
+        in_specs=[vmem] * 3 + [pl.BlockSpec(memory_space=pltpu.SMEM)] + [vmem] * 4 + [hbm] * 3,
+        out_specs=(vmem, hbm, hbm, hbm, hbm),
         scratch_shapes=[
             pltpu.VMEM((shards * rows, width), jnp.bfloat16),
             pltpu.VMEM((shards * rows, width), jnp.bfloat16),
@@ -396,24 +475,34 @@
             pltpu.VMEM(w_gate.shape, jnp.bfloat16),
             pltpu.VMEM(w_up.shape, jnp.bfloat16),
             pltpu.VMEM(w_down.shape, jnp.bfloat16),
+            pltpu.VMEM((rows, width), jnp.bfloat16),
+            pltpu.VMEM((rows // 2, width), jnp.bfloat16),
+            pltpu.VMEM(resid.shape, jnp.float32),
+            pltpu.VMEM(resid.shape, jnp.bfloat16),
             pltpu.SemaphoreType.DMA((2, 5, shards)),
             pltpu.SemaphoreType.DMA((2, shards)),
             pltpu.SemaphoreType.DMA((3, 4, shards)),
             pltpu.SemaphoreType.DMA((3, shards)),
             pltpu.SemaphoreType.DMA((3,)),
             pltpu.SemaphoreType.DMA((3,)),
+            pltpu.SemaphoreType.DMA((3,)),
+            pltpu.SemaphoreType.DMA((3,)),
+            pltpu.SemaphoreType.DMA((2, 2)),
         ],
         compiler_params=pltpu.CompilerParams(collective_id=0, has_side_effects=True),
         name="front",
-    )(queries, keys, values, score_shift, w_gate, w_up, w_down)
+    )(
+        queries, keys, values, score_shift, resid, w_out, gain_mix[None], gain_pre[None],
+        w_gate, w_up, w_down,
+    )
 
 
 def local(
     queries, keys, values, score_shift, resid, w_out, gain_mix, gain_pre,
     w_gate, w_up, conv_gate, conv_up, w_down, gain_post,
 ):
-    attended, gate_w, up_w, down_w = front(
-        queries, keys, values, score_shift, w_gate, w_up, w_down
+    middle, tokens, gate_w, up_w, down_w = front(
+        queries, keys, values, score_shift, resid, w_out, gain_mix, gain_pre, w_gate, w_up, w_down
     )
     shards = lax.axis_size("sp")
     hop = shards // 2
@@ -421,18 +510,7 @@
     half = sp // hop
     units = gate_w.shape[1]
     pairs = [(i, (i + hop) % shards) for i in range(shards)]
-    head_rows = lax.all_to_all(attended, "tp", split_axis=0, concat_axis=1, tiled=True)
-    mixed = jnp.dot(head_rows, w_out, preferred_element_type=jnp.float32).astype(jnp.bfloat16)
-    middle = (resid.astype(jnp.float32) + gain_mix * rms_scale(mixed.astype(jnp.float32))).astype(
-        jnp.bfloat16
-    )
-    normed = (gain_pre * rms_scale(middle.astype(jnp.float32))).astype(jnp.bfloat16)
-    piece = lax.all_gather(normed, "tp", axis=0, tiled=True)
-    other = lax.ppermute(piece, "sp", pairs)
-    run = piece.shape[0]
-    tokens = jnp.where(
-        half == 0, jnp.concatenate([piece, other], 0), jnp.concatenate([other, piece], 0)
-    )
+    run = tokens.shape[0] // 2
     conv_g = lax.dynamic_slice_in_dim(conv_gate, half * units, units, 1)
     conv_u = lax.dynamic_slice_in_dim(conv_up, half * units, units, 1)
     gate_part = jnp.dot(tokens, gate_w, preferred_element_type=jnp.float32).astype(jnp.bfloat16)

time: 359 us -> 284 us (0.79)
  waiting for transfers between devices: 180 us -> 67.5 us
  Pallas kernels: 116 us -> 177 us
  blocking collectives: 7.06 us -> 0 us
  local copies, waits for them, and re-layouts: 7.71 us -> 2.84 us
  matrix products: 19.1 us -> 14.6 us
  starting transfers between devices: 4.45 us -> 0.25 us
    all_gather x1 -> x0, waiting for transfers between devices: 66.6 us -> none  [local(): piece = lax.all_gather(normed, 'tp', axis=0, tiled=True)]
    pallas_call x1, Pallas kernels: 116 us -> 177 us  [front(): pl.pallas_call(front_kernel, out_shape=(jax.ShapeDtypeStruct(resid.shape,...]
    ppermute x1 -> x0, waiting for transfers between devices: 45 us -> none  [local(): other = lax.ppermute(piece, 'sp', pairs)]
    all_to_all x1 -> x0, blocking collectives: 7.06 us -> none  [local(): lax.all_to_all(attended, 'tp', split_axis=0, concat_axis=1, tiled=True)]
    dot_general x1, matrix products: 7.4 us -> 3.41 us  [local(): jnp.dot(tokens, gate_w, preferred_element_type=jnp.float32)]
  transfers between devices with their start and end apart: 5 -> 3, of which waited for: 5 -> 3; matrix products, arithmetic and copies ran while one was open for 0% -> 0% of each run, Pallas kernels for 0% -> 0%
where the time goes in v2:
time: 284 us
  Pallas kernels  177 us (62%)
  waiting for transfers between devices  67.5 us (24%)
  matrix products  14.6 us (5%)
  between operations  13.6 us (5%)
  other arithmetic  8.33 us (3%)
  local copies, waits for them, and re-layouts  2.84 us (1%)
    pallas_call x1, Pallas kernels, front(): pl.pallas_call(front_kernel, out_shape=(jax.ShapeDtypeStruct(resid.shape,...  177 us
    ppermute x1, waiting for transfers between devices, local(): back = lax.ppermute(away, 'sp', pairs)  45.7 us
    reduce_scatter x1, waiting for transfers between devices, local(): summed = lax.psum_scatter(both, 'tp', scatter_dimension=0, tiled=True)  18.9 us
    dot_general x1, matrix products, local(): jnp.dot(tokens, up_w, preferred_element_type=jnp.float32)  6.82 us
  transfers between devices with their start and end apart: 3, of which 3 were waited for; matrix products, arithmetic and copies ran while one was open for 0% of the time, Pallas kernels for 0%

profile of v2, /device:TPU:0, one launch (start us, length us, event | category | flops | bytes accessed | tf_op | source)
XLA Modules:
  0.0 283.9 jit_solution(10582250414901002231)
XLA Ops:
  6.5 0.0 reduce-scatter.2.cloned.1.call-start
  6.5 176.7 %front.1 = (bf16[128,2048]{1,0:T(8,128)(2,1)}, bf16[512,2048]{1,0:T(8,128)(2,1)}, bf16[2048,1408]{1,0:T(8,128)(2,1)}, bf16[2048,1408]{1,0:T(8,128)(2,1)}, bf16[1408,2048]{1,0:T(8,128)(2,1)}) custom-call(bf16[256,256]{1,0:T(8,128)(2,1)} %q_ref.1, bf16[256,256]{1,0:T(8,128)(2,1)} %k_ref.1, bf16[256,256]{1,0:T(8,128)(2,1)} %v_ref.1, f32[4]{0:T(128)} %shift_ref.1, ...), custom_call_target="tpu_custom_call" | custom-call | tf_op jit(solution)/shard_map/front/pallas_call | solution.py:457
  183.3 0.0 copy-start.2
  183.3 0.0 copy-start.3
  183.3 6.8 %convolution_convert_fusion = bf16[512,1408]{1,0:T(8,128)(2,1)S(1)} fusion(bf16[512,2048]{1,0:T(8,128)(2,1)} %get-tuple-element.11, bf16[2048,1408]{1,0:T(8,128)(2,1)} %get-tuple-element.13), kind=kOutput, calls=%fused_computation | convolution fusion | flops 2953510912 | bytes 9306112 | tf_op jit(solution)/shard_map/dot_general | solution.py:517
  190.1 0.0 copy-done.2
  190.2 0.0 copy-done.3
  190.2 3.4 %convolution_convert_fusion.1 = bf16[512,1408]{1,0:T(8,128)(2,1)S(1)} fusion(bf16[512,2048]{1,0:T(8,128)(2,1)S(1)} %copy-done.3, bf16[2048,1408]{1,0:T(8,128)(2,1)S(1)} %copy-done.2), kind=kOutput, calls=%fused_computation.1 | convolution fusion | flops 2953510912 | bytes 9306112 | tf_op jit(solution)/shard_map/dot_general | solution.py:516
  193.7 0.1 collective-permute-start
  193.8 0.1 fusion.18
  193.9 0.1 fusion.17
  194.0 1.0 dynamic-slice_reduce_fusion.2
  195.0 2.9 %collective-permute-done = bf16[2,2,2,1408]{3,2,1,0:T(2,128)(2,1)S(1)} collective-permute-done((bf16[2,2,2,1408]{3,2,1,0:T(2,128)(2,1)S(1)}, bf16[2,2,2,1408]{3,2,1,0:T(2,128)(2,1)S(1)}, u32[]{:S(2)}, u32[]{:S(2)}) %collective-permute-start) | collective-permute-done | bytes 22560 | tf_op jit(solution)/shard_map/ppermute | solution.py:526
  198.0 0.3 maximum_convert_fusion.2
  198.3 0.3 maximum_convert_fusion
  198.6 0.0 slice-start
  198.6 0.8 fusion.4
  199.4 0.0 slice-start.1
  199.4 0.8 fusion.8
  200.3 0.0 slice-done
  200.3 1.4 slice-done.1
  201.7 4.3 %convolution_convert_fusion.2 = bf16[512,2048]{1,0:T(8,128)(2,1)S(1)} fusion(bf16[1408,2048]{1,0:T(8,128)(2,1)S(1)} %bitcast.30, f32[256,1408]{1,0:T(8,128)S(1)} %get-tuple-element.32, f32[256,1408]{1,0:T(8,128)S(1)} %get-tuple-element.31, f32[256,1408]{1,0:T(8,128)S(1)} %get-tuple-element.30, f32[256,1408]{1,0:T(8,128)S(1)} %get-tuple-element.29), kind=kOutput, calls=%fused_computation.2 | convolution fusion | flops 2959605760 | bytes 13631488 | tf_op jit(solution)/shard_map/dot_general | solution.py:545
  206.1 0.1 constant_dynamic-slice_fusion
  206.2 0.2 collective-permute-start.1
  206.4 45.7 %collective-permute-done.1 = bf16[256,2048]{1,0:T(8,128)(2,1)} collective-permute-done((bf16[256,2048]{1,0:T(8,128)(2,1)S(1)}, bf16[256,2048]{1,0:T(8,128)(2,1)}, u32[]{:S(2)}, u32[]{:S(2)}) %collective-permute-start.1) | collective-permute-done | bytes 1048608 | tf_op jit(solution)/shard_map/ppermute | solution.py:548
  252.1 2.6 add_convert_fusion
  254.7 0.0 reduce-scatter.2.cloned.1.call-update
  254.8 18.9 %reduce-scatter.2.cloned.1.call-done = bf16[128,2048]{1,0:T(8,128)(2,1)} async-done(((bf16[256,2048]{1,0:T(8,128)(2,1)}), bf16[128,2048]{1,0:T(8,128)(2,1)}) %reduce-scatter.2.cloned.1.call-update) | async-done | bytes 524304 | tf_op jit(solution)/shard_map/reduce_scatter | solution.py:550
  273.7 1.2 fusion.11
  274.9 0.0 copy-done
  274.9 0.0 copy-done.1
  275.0 2.1 fusion.14
  (12 shorter events, 0.2 us)
Async XLA Ops:
  6.5 267.2 %reduce-scatter.2.cloned.1.call-start = ((), (), s32[]{:S(2)}) async-start(), calls=%async_computation.1 | async-start | bytes 1572864 | tf_op jit(solution)/shard_map/reduce_scatter | solution.py:550
  183.3 6.9 %copy-start.2 = (bf16[2048,1408]{1,0:T(8,128)(2,1)S(1)}, bf16[2048,1408]{1,0:T(8,128)(2,1)}, u32[]{:S(2)}) copy-start(bf16[2048,1408]{1,0:T(8,128)(2,1)} %get-tuple-element.12) | copy-start | bytes 17301508
  183.3 6.9 %copy-start.3 = (bf16[512,2048]{1,0:T(8,128)(2,1)S(1)}, bf16[512,2048]{1,0:T(8,128)(2,1)}, u32[]{:S(2)}) copy-start(bf16[512,2048]{1,0:T(8,128)(2,1)} %get-tuple-element.11) | copy-start | bytes 6291460
  193.7 4.2 %collective-permute-start = (bf16[2,2,2,1408]{3,2,1,0:T(2,128)(2,1)S(1)}, bf16[2,2,2,1408]{3,2,1,0:T(2,128)(2,1)S(1)}, u32[]{:S(2)}, u32[]{:S(2)}) collective-permute-start(bf16[2,2,2,1408]{3,2,1,0:T(2,128)(2,1)S(1)} %pad_maximum_fusion.1), channel_id=1, source_target_pairs={{0,2},{2,4},{4,6},{6,8},{8,10},{10,12},{12,14},{14,0},{16,18},{18,... | collective-permute-start | bytes 67592 | tf_op jit(solution)/shard_map/ppermute | solution.py:526
  198.6 1.7 slice-start
  199.4 2.3 slice-start.1
  206.2 45.9 %collective-permute-start.1 = (bf16[256,2048]{1,0:T(8,128)(2,1)S(1)}, bf16[256,2048]{1,0:T(8,128)(2,1)}, u32[]{:S(2)}, u32[]{:S(2)}) collective-permute-start(bf16[256,2048]{1,0:T(8,128)(2,1)S(1)} %constant_dynamic-slice_fusion), channel_id=1, source_target_pairs={{0,16},{2,18},{4,20},{6,22},{8,24},{10,26},{12,28},{14,30},{16,0},... | collective-permute-start | bytes 3145736 | tf_op jit(solution)/shard_map/ppermute | solution.py:548
  254.7 20.2 %copy-start = (bf16[128,2048]{1,0:T(8,128)(2,1)S(1)}, bf16[128,2048]{1,0:T(8,128)(2,1)}, u32[]{:S(2)}) copy-start(bf16[128,2048]{1,0:T(8,128)(2,1)} %get-tuple-element.10) | copy-start | bytes 1572868
  254.7 20.2 %copy-start.1 = (f32[2048]{0:T(1024)S(1)}, f32[2048]{0:T(1024)}, u32[]{:S(2)}) copy-start(f32[2048]{0:T(1024)} %param.27) | copy-start | bytes 24580
Sparse Core Ops, SparseCore 0:
  254.9 18.7 reduce-scatter.1

commit v3 on v2

--- a/solution.py
+++ b/solution.py
@@ -497,6 +497,112 @@
     )
 
 
+def back_kernel(
+    hid_ref, down_ref, mid_ref, post_ref, out_ref,
+    own, out_x, in_x, out_z, in_z, x_send, x_recv, z_send, z_recv,
+):
+    rows, wide = mid_ref.shape
+    parts = x_recv.shape[1]
+    step_cols = wide // parts
+    shards = NZ * NY * NC
+    hop = shards // 2
+    sp, tp = lax.axis_index("sp"), lax.axis_index("tp")
+    half = sp // hop
+    pair = lax.rem(sp + hop, shards)
+
+    barrier = pltpu.get_barrier_semaphore()
+    pl.semaphore_signal(barrier, inc=1, device_id={"tp": 1 - tp}, device_id_type=MESH)
+    pl.semaphore_signal(barrier, inc=1, device_id={"sp": pair}, device_id_type=MESH)
+    pl.semaphore_wait(barrier, 2)
+
+    def block(part, xx):
+        return hid_ref[pl.ds(pl.multiple_of((part * 2 + xx) * rows, rows), rows), :]
+
+    def along_x(i, n):
+        chunk = pl.ds(n * step_cols, step_cols)
+        return pltpu.make_async_remote_copy(
+            src_ref=out_x.at[i, :, chunk], dst_ref=in_x.at[i, :, chunk],
+            send_sem=x_send.at[i, n], recv_sem=x_recv.at[i, n],
+            device_id={"tp": 1 - tp}, device_id_type=MESH,
+        )
+
+    def along_z(n):
+        chunk = pl.ds(n * step_cols, step_cols)
+        return pltpu.make_async_remote_copy(
+            src_ref=out_z.at[:, chunk], dst_ref=in_z.at[:, chunk],
+            send_sem=z_send.at[n], recv_sem=z_recv.at[n],
+            device_id={"sp": pair}, device_id_type=MESH,
+        )
+
+    def product(lhs, n):
+        return jnp.dot(
+            lhs, down_ref[:, n * step_cols : (n + 1) * step_cols],
+            preferred_element_type=jnp.float32,
+        ).astype(jnp.bfloat16)
+
+    theirs = jnp.concatenate([block(1 - half, 1 - tp), block(half, 1 - tp)], axis=0)
+    for n in range(parts):
+        value = product(theirs, n)
+        out_x[0, :, n * step_cols : (n + 1) * step_cols] = value[:rows]
+        out_x[1, :, n * step_cols : (n + 1) * step_cols] = value[rows:]
+        along_x(0, n).start()
+    for n in range(parts):
+        along_x(1, n).start()
+    mine = jnp.concatenate([block(1 - half, tp), block(half, tp)], axis=0)
+    for n in range(parts):
+        value = product(mine, n)
+        own[0, :, n * step_cols : (n + 1) * step_cols] = value[:rows]
+        own[1, :, n * step_cols : (n + 1) * step_cols] = value[rows:]
+    for n in range(parts):
+        chunk = pl.ds(n * step_cols, step_cols)
+        along_x(0, n).wait_recv()
+        out_z[:, chunk] = (
+            own[0, :, chunk].astype(jnp.float32) + in_x[0, :, chunk].astype(jnp.float32)
+        ).astype(jnp.bfloat16)
+        along_z(n).start()
+    for n in range(parts):
+        along_x(1, n).wait_recv()
+    for n in range(parts):
+        along_z(n).wait_recv()
+
+    @pl.loop(0, rows // 16)
+    def _(i):
+        part = pl.ds(pl.multiple_of(i * 16, 16), 16)
+        total = own[1, part, :].astype(jnp.float32) + in_x[1, part, :].astype(jnp.float32)
+        total = (total + in_z[part, :].astype(jnp.float32)).astype(jnp.bfloat16)
+        out_ref[part, :] = (
+            mid_ref[part, :].astype(jnp.float32)
+            + post_ref[...] * rms_scale(total.astype(jnp.float32))
+        ).astype(jnp.bfloat16)
+
+    for n in range(parts):
+        along_x(0, n).wait_send()
+        along_x(1, n).wait_send()
+        along_z(n).wait_send()
+
+
+def back(hidden, down_w, middle, gain_post):
+    vmem = pl.BlockSpec(memory_space=pltpu.VMEM)
+    parts = 4
+    pair = pltpu.VMEM((2,) + middle.shape, jnp.bfloat16)
+    one = pltpu.VMEM(middle.shape, jnp.bfloat16)
+    return pl.pallas_call(
+        back_kernel,
+        out_shape=jax.ShapeDtypeStruct(middle.shape, jnp.bfloat16),
+        in_specs=[vmem] * 4,
+        out_specs=vmem,
+        scratch_shapes=[
+            pair, pair, pair, one, one,
+            pltpu.SemaphoreType.DMA((2, parts)),
+            pltpu.SemaphoreType.DMA((2, parts)),
+            pltpu.SemaphoreType.DMA((parts,)),
+            pltpu.SemaphoreType.DMA((parts,)),
+        ],
+        compiler_params=pltpu.CompilerParams(collective_id=1, has_side_effects=True),
+        name="back",
+    )(hidden, down_w, middle, gain_post[None])
+
+
 def local(
     queries, keys, values, score_shift, resid, w_out, gain_mix, gain_pre,
     w_gate, w_up, conv_gate, conv_up, w_down, gain_post,
@@ -509,7 +615,6 @@
     sp = lax.axis_index("sp")
     half = sp // hop
     units = gate_w.shape[1]
-    pairs = [(i, (i + hop) % shards) for i in range(shards)]
     run = tokens.shape[0] // 2
     conv_g = lax.dynamic_slice_in_dim(conv_gate, half * units, units, 1)
     conv_u = lax.dynamic_slice_in_dim(conv_up, half * units, units, 1)
@@ -542,15 +647,7 @@
     hidden = (
         jax.nn.silu(convolve(gate_part, before[0], conv_g)) * convolve(up_part, before[1], conv_u)
     ).astype(jnp.bfloat16)
-    partial = jnp.dot(hidden, down_w, preferred_element_type=jnp.float32).astype(jnp.bfloat16)
-    away = lax.dynamic_slice_in_dim(partial, (1 - half) * run, run, 0)
-    mine = lax.dynamic_slice_in_dim(partial, half * run, run, 0)
-    back = lax.ppermute(away, "sp", pairs)
-    both = (mine.astype(jnp.float32) + back.astype(jnp.float32)).astype(jnp.bfloat16)
-    summed = lax.psum_scatter(both, "tp", scatter_dimension=0, tiled=True)
-    return (middle.astype(jnp.float32) + gain_post * rms_scale(summed.astype(jnp.float32))).astype(
-        jnp.bfloat16
-    )
+    return back(hidden, down_w, middle, gain_post)
 
 
 def solution(mesh):

time: 284 us -> 231 us (0.81)
  waiting for transfers between devices: 67.5 us -> 2.84 us
  Pallas kernels: 177 us -> 210 us
  between operations: 13.6 us -> 0.2 us
  matrix products: 14.6 us -> 10.2 us
  other arithmetic: 8.33 us -> 4.39 us
    ppermute x1 -> x0, waiting for transfers between devices: 45.7 us -> none  [local(): back = lax.ppermute(away, 'sp', pairs)]
    pallas_call x0 -> x1, Pallas kernels: none -> 33 us  [back(): pl.pallas_call(back_kernel, out_shape=jax.ShapeDtypeStruct(middle.shape,...]
    reduce_scatter x1 -> x0, waiting for transfers between devices: 18.9 us -> none  [local(): summed = lax.psum_scatter(both, 'tp', scatter_dimension=0, tiled=True)]
    dot_general x1 -> x0, matrix products: 4.33 us -> none  [local(): jnp.dot(hidden, down_w, preferred_element_type=jnp.float32)]
  transfers between devices with their start and end apart: 3 -> 1, of which waited for: 3 -> 1; matrix products, arithmetic and copies ran while one was open for 0% -> 1% of each run, Pallas kernels for 0% -> 0%
where the time goes in v3:
time: 231 us
  Pallas kernels  210 us (91%)
  matrix products  10.2 us (4%)
  other arithmetic  4.39 us (2%)
  local copies, waits for them, and re-layouts  3.17 us (1%)
  waiting for transfers between devices  2.84 us (1%)
    pallas_call x1, Pallas kernels, front(): pl.pallas_call(front_kernel, out_shape=(jax.ShapeDtypeStruct(resid.shape,...  177 us
    pallas_call x1, Pallas kernels, back(): pl.pallas_call(back_kernel, out_shape=jax.ShapeDtypeStruct(middle.shape,...  33 us
    dot_general x1, matrix products, local(): jnp.dot(tokens, up_w, preferred_element_type=jnp.float32)  6.82 us
  transfers between devices with their start and end apart: 1, of which 1 were waited for; matrix products, arithmetic and copies ran while one was open for 1% of the time, Pallas kernels for 0%

profile of v3, /device:TPU:0, one launch (start us, length us, event | category | flops | bytes accessed | tf_op | source)
XLA Modules:
  0.0 230.7 jit_solution(10552097437468709825)
XLA Ops:
  0.0 176.7 %front.1 = (bf16[128,2048]{1,0:T(8,128)(2,1)}, bf16[512,2048]{1,0:T(8,128)(2,1)}, bf16[2048,1408]{1,0:T(8,128)(2,1)}, bf16[2048,1408]{1,0:T(8,128)(2,1)}, bf16[1408,2048]{1,0:T(8,128)(2,1)}) custom-call(bf16[256,256]{1,0:T(8,128)(2,1)} %q_ref.1, bf16[256,256]{1,0:T(8,128)(2,1)} %k_ref.1, bf16[256,256]{1,0:T(8,128)(2,1)} %v_ref.1, f32[4]{0:T(128)} %shift_ref.1, ...), custom_call_target="tpu_custom_call" | custom-call | tf_op jit(solution)/shard_map/front/pallas_call | solution.py:457
  176.7 0.0 copy-start
  176.8 0.0 copy-start.1
  176.8 6.8 %convolution_convert_fusion = bf16[512,1408]{1,0:T(8,128)(2,1)S(1)} fusion(bf16[512,2048]{1,0:T(8,128)(2,1)} %get-tuple-element.10, bf16[2048,1408]{1,0:T(8,128)(2,1)} %get-tuple-element.12), kind=kOutput, calls=%fused_computation | convolution fusion | flops 2953510912 | bytes 9306112 | tf_op jit(solution)/shard_map/dot_general | solution.py:622
  183.6 0.0 copy-done
  183.6 0.0 copy-done.1
  183.6 3.4 %convolution_convert_fusion.1 = bf16[512,1408]{1,0:T(8,128)(2,1)S(1)} fusion(bf16[512,2048]{1,0:T(8,128)(2,1)S(1)} %copy-done.1, bf16[2048,1408]{1,0:T(8,128)(2,1)S(1)} %copy-done), kind=kOutput, calls=%fused_computation.1 | convolution fusion | flops 2953510912 | bytes 9306112 | tf_op jit(solution)/shard_map/dot_general | solution.py:621
  187.2 0.1 collective-permute-start
  187.2 0.1 fusion.10
  187.4 0.1 fusion.9
  187.5 1.0 dynamic-slice_reduce_fusion.2
  188.5 2.8 %collective-permute-done = bf16[2,2,2,1408]{3,2,1,0:T(2,128)(2,1)S(1)} collective-permute-done((bf16[2,2,2,1408]{3,2,1,0:T(2,128)(2,1)S(1)}, bf16[2,2,2,1408]{3,2,1,0:T(2,128)(2,1)S(1)}, u32[]{:S(2)}, u32[]{:S(2)}) %collective-permute-start) | collective-permute-done | bytes 22560 | tf_op jit(solution)/shard_map/ppermute | solution.py:631
  191.4 0.3 maximum_convert_fusion.2
  191.7 0.3 maximum_convert_fusion
  192.0 0.8 fusion.3
  192.9 0.8 fusion.7
  193.7 2.0 fusion.hid_ref
  195.7 33.0 %back.1 = bf16[128,2048]{1,0:T(8,128)(2,1)} custom-call(bf16[512,1408]{1,0:T(8,128)(2,1)} %fusion.hid_ref, bf16[1408,2048]{1,0:T(8,128)(2,1)} %get-tuple-element.13.down_ref, bf16[128,2048]{1,0:T(8,128)(2,1)} %get-tuple-element.14.mid_ref, f32[1,2048]{1,0:T(1,128)} %bitcast.29), custom_call_target="tpu_custom_call" | custom-call | tf_op jit(solution)/shard_map/back/pallas_call | solution.py:589
  228.8 1.9 copy.16
  (8 shorter events, 0.2 us)
Async XLA Ops:
  176.7 6.9 %copy-start = (bf16[2048,1408]{1,0:T(8,128)(2,1)S(1)}, bf16[2048,1408]{1,0:T(8,128)(2,1)}, u32[]{:S(2)}) copy-start(bf16[2048,1408]{1,0:T(8,128)(2,1)} %get-tuple-element.11) | copy-start | bytes 17301508
  176.8 6.9 %copy-start.1 = (bf16[512,2048]{1,0:T(8,128)(2,1)S(1)}, bf16[512,2048]{1,0:T(8,128)(2,1)}, u32[]{:S(2)}) copy-start(bf16[512,2048]{1,0:T(8,128)(2,1)} %get-tuple-element.10) | copy-start | bytes 6291460
  187.2 4.2 %collective-permute-start = (bf16[2,2,2,1408]{3,2,1,0:T(2,128)(2,1)S(1)}, bf16[2,2,2,1408]{3,2,1,0:T(2,128)(2,1)S(1)}, u32[]{:S(2)}, u32[]{:S(2)}) collective-permute-start(bf16[2,2,2,1408]{3,2,1,0:T(2,128)(2,1)S(1)} %pad_maximum_fusion.1), channel_id=1, source_target_pairs={{0,2},{2,4},{4,6},{6,8},{8,10},{10,12},{12,14},{14,0},{16,18},{18,... | collective-permute-start | bytes 67592 | tf_op jit(solution)/shard_map/ppermute | solution.py:631

commit v4 on v3

--- a/solution.py
+++ b/solution.py
@@ -240,7 +240,7 @@
         qs[h] = jnp.where(lane_head == h, q_all, 0.0).astype(jnp.bfloat16)
     r_idx = lax.broadcasted_iota(jnp.int32, (rows, rows), 0)
     c_idx = lax.broadcasted_iota(jnp.int32, (rows, rows), 1)
-    tri[...] = jnp.where(r_idx > c_idx, 1.0, 0.0).astype(jnp.bfloat16)
+    tri[...] = jnp.where(r_idx > c_idx, -1.0, 0.0).astype(jnp.bfloat16)
     acc[...] = jnp.zeros_like(acc)
     tail[...] = jnp.zeros_like(tail)
 
@@ -249,12 +249,12 @@
             scores = lax.dot_general(
                 qs[h], kb, (((1,), (1,)), ((), ())), preferred_element_type=jnp.float32
             ) - shift_ref[h]
-            keep = -(jnp.maximum(scores, 0.0) + jnp.log(1.0 + jnp.exp(-jnp.abs(scores))))
-            take = scores + keep
+            drop = jnp.maximum(scores, 0.0) + jnp.log(1.0 + jnp.exp(-jnp.abs(scores)))
+            take = scores - drop
             if masked:
-                keep = jnp.where(c_idx < r_idx, keep, 0.0)
-            high = keep.astype(jnp.bfloat16)
-            low = (keep - high.astype(jnp.float32)).astype(jnp.bfloat16)
+                drop = jnp.where(c_idx < r_idx, drop, 0.0)
+            high = drop.astype(jnp.bfloat16)
+            low = (drop - high.astype(jnp.float32)).astype(jnp.bfloat16)
             later = jnp.dot(high, tri[...], preferred_element_type=jnp.float32) + jnp.dot(
                 low, tri[...], preferred_element_type=jnp.float32
             )
@@ -263,7 +263,7 @@
             if masked:
                 weights = jnp.where(c_idx < r_idx, weights, 0.0)
             acc[h] += jnp.dot(weights.astype(jnp.bfloat16), vb, preferred_element_type=jnp.float32)
-            tail[h] = before + (later[:, 0:1] + keep[:, 0:1])
+            tail[h] = before + (later[:, 0:1] - drop[:, 0:1])
 
     attend(k_ref[...], v_ref[...], True)
 
@@ -325,6 +325,7 @@
         arrived(cross_out, True)
     @pl.when(z >= 3)
     def _():
+        arrived(cross_in, False)
         plane(3)
 
     total = jnp.zeros((rows, width), jnp.float32)
@@ -341,7 +342,7 @@
     )
     swap.start()
 
-    @pl.when(jnp.logical_not(inner))
+    @pl.when(z == 0)
     def _():
         arrived(cross_in, False)
 

time: 231 us -> 240 us (1.039)
  waiting for transfers between devices: 2.84 us -> 13.1 us
    pallas_call x1, Pallas kernels: 177 us -> 165 us  [front(): pl.pallas_call(front_kernel, out_shape=(jax.ShapeDtypeStruct(resid.shape,...]
    pallas_call x1, Pallas kernels: 33 us -> 43.3 us  [back(): pl.pallas_call(back_kernel, out_shape=jax.ShapeDtypeStruct(middle.shape,...]
    ppermute x1, waiting for transfers between devices: 2.84 us -> 13.1 us  [local(): before = lax.ppermute(edges, 'sp', ring)]
where the time goes in v4:
time: 240 us
  Pallas kernels  209 us (87%)
  waiting for transfers between devices  13.1 us (5%)
  matrix products  10.2 us (4%)
  other arithmetic  4.39 us (2%)
  local copies, waits for them, and re-layouts  3.17 us (1%)
    pallas_call x1, Pallas kernels, front(): pl.pallas_call(front_kernel, out_shape=(jax.ShapeDtypeStruct(resid.shape,...  165 us
    pallas_call x1, Pallas kernels, back(): pl.pallas_call(back_kernel, out_shape=jax.ShapeDtypeStruct(middle.shape,...  43.3 us
    ppermute x1, waiting for transfers between devices, local(): before = lax.ppermute(edges, 'sp', ring)  13.1 us
    dot_general x1, matrix products, local(): jnp.dot(tokens, up_w, preferred_element_type=jnp.float32)  6.82 us
  transfers between devices with their start and end apart: 1, of which 1 were waited for; matrix products, arithmetic and copies ran while one was open for 1% of the time, Pallas kernels for 0%

profile of v4, /device:TPU:0, one launch (start us, length us, event | category | flops | bytes accessed | tf_op | source)
XLA Modules:
  0.0 239.7 jit_solution(4241091017057676256)
XLA Ops:
  0.0 165.2 %front.1 = (bf16[128,2048]{1,0:T(8,128)(2,1)}, bf16[512,2048]{1,0:T(8,128)(2,1)}, bf16[2048,1408]{1,0:T(8,128)(2,1)}, bf16[2048,1408]{1,0:T(8,128)(2,1)}, bf16[1408,2048]{1,0:T(8,128)(2,1)}) custom-call(bf16[256,256]{1,0:T(8,128)(2,1)} %q_ref.1, bf16[256,256]{1,0:T(8,128)(2,1)} %k_ref.1, bf16[256,256]{1,0:T(8,128)(2,1)} %v_ref.1, f32[4]{0:T(128)} %shift_ref.1, ...), custom_call_target="tpu_custom_call" | custom-call | tf_op jit(solution)/shard_map/front/pallas_call | solution.py:458
  165.3 0.0 copy-start
  165.3 0.0 copy-start.1
  165.3 6.8 %convolution_convert_fusion = bf16[512,1408]{1,0:T(8,128)(2,1)S(1)} fusion(bf16[512,2048]{1,0:T(8,128)(2,1)} %get-tuple-element.10, bf16[2048,1408]{1,0:T(8,128)(2,1)} %get-tuple-element.12), kind=kOutput, calls=%fused_computation | convolution fusion | flops 2953510912 | bytes 9306112 | tf_op jit(solution)/shard_map/dot_general | solution.py:623
  172.1 0.0 copy-done
  172.1 0.0 copy-done.1
  172.1 3.4 %convolution_convert_fusion.1 = bf16[512,1408]{1,0:T(8,128)(2,1)S(1)} fusion(bf16[512,2048]{1,0:T(8,128)(2,1)S(1)} %copy-done.1, bf16[2048,1408]{1,0:T(8,128)(2,1)S(1)} %copy-done), kind=kOutput, calls=%fused_computation.1 | convolution fusion | flops 2953510912 | bytes 9306112 | tf_op jit(solution)/shard_map/dot_general | solution.py:622
  175.7 0.1 collective-permute-start
  175.8 0.1 fusion.10
  175.9 0.1 fusion.9
  176.0 1.0 dynamic-slice_reduce_fusion.2
  177.0 13.1 %collective-permute-done = bf16[2,2,2,1408]{3,2,1,0:T(2,128)(2,1)S(1)} collective-permute-done((bf16[2,2,2,1408]{3,2,1,0:T(2,128)(2,1)S(1)}, bf16[2,2,2,1408]{3,2,1,0:T(2,128)(2,1)S(1)}, u32[]{:S(2)}, u32[]{:S(2)}) %collective-permute-start) | collective-permute-done | bytes 22560 | tf_op jit(solution)/shard_map/ppermute | solution.py:632
  190.2 0.3 maximum_convert_fusion.2
  190.5 0.3 maximum_convert_fusion
  190.8 0.8 fusion.3
  191.7 0.8 fusion.7
  192.5 2.0 fusion.hid_ref
  194.5 43.3 %back.1 = bf16[128,2048]{1,0:T(8,128)(2,1)} custom-call(bf16[512,1408]{1,0:T(8,128)(2,1)} %fusion.hid_ref, bf16[1408,2048]{1,0:T(8,128)(2,1)} %get-tuple-element.13.down_ref, bf16[128,2048]{1,0:T(8,128)(2,1)} %get-tuple-element.14.mid_ref, f32[1,2048]{1,0:T(1,128)} %bitcast.29), custom_call_target="tpu_custom_call" | custom-call | tf_op jit(solution)/shard_map/back/pallas_call | solution.py:590
  237.8 1.9 copy.16
  (8 shorter events, 0.2 us)
Async XLA Ops:
  165.3 6.9 %copy-start = (bf16[2048,1408]{1,0:T(8,128)(2,1)S(1)}, bf16[2048,1408]{1,0:T(8,128)(2,1)}, u32[]{:S(2)}) copy-start(bf16[2048,1408]{1,0:T(8,128)(2,1)} %get-tuple-element.11) | copy-start | bytes 17301508
  165.3 6.9 %copy-start.1 = (bf16[512,2048]{1,0:T(8,128)(2,1)S(1)}, bf16[512,2048]{1,0:T(8,128)(2,1)}, u32[]{:S(2)}) copy-start(bf16[512,2048]{1,0:T(8,128)(2,1)} %get-tuple-element.10) | copy-start | bytes 6291460
  175.7 14.4 %collective-permute-start = (bf16[2,2,2,1408]{3,2,1,0:T(2,128)(2,1)S(1)}, bf16[2,2,2,1408]{3,2,1,0:T(2,128)(2,1)S(1)}, u32[]{:S(2)}, u32[]{:S(2)}) collective-permute-start(bf16[2,2,2,1408]{3,2,1,0:T(2,128)(2,1)S(1)} %pad_maximum_fusion.1), channel_id=1, source_target_pairs={{0,2},{2,4},{4,6},{6,8},{8,10},{10,12},{12,14},{14,0},{16,18},{18,... | collective-permute-start | bytes 67592 | tf_op jit(solution)/shard_map/ppermute | solution.py:632
